TPU v7x, 32 devices: a whole 2x2x4 slice. The times are simulated.
32 devices in a mesh: fs: 8 (over z, x), tp: 4 (over y, core).
Axes of the slice: x: 2, y: 2, z: 4, core: 2. Of those that a mesh axis runs over, the one named last changes fastest.
Arguments:
- tokens: bfloat16 [8192, 2048], P('fs', 'tp'), may hold values from -6 to 6
- grad_out: bfloat16 [8192, 2048], P('fs', 'tp'), may hold values from -6 to 6
- norm_gain: float32 [2048], replicated, may hold values from 0.1 to 1.9
- gate_weight: bfloat16 [3072, 2048], P('tp', 'fs'), may hold values from -0.125 to 0.125
- up_weight: bfloat16 [3072, 2048], P('tp', 'fs'), may hold values from -0.125 to 0.125
- down_weight: bfloat16 [3072, 2048], P('tp', 'fs'), may hold values from -0.109375 to 0.109375
Outputs:
- grad_input: bfloat16 [8192, 2048], P('fs', 'tp')
- grad_gate: float32 [3072, 2048], P('tp', 'fs')
- grad_up: float32 [3072, 2048], P('tp', 'fs')
- grad_down: float32 [3072, 2048], P('tp', 'fs')
- row_squares: float32 [3, 3072], P(None, 'tp')
All inputs are finite; a program needn't handle non-finite values.
Results may differ from a plain program's by a relative error of at most 0.015.
Values may be sent and summed in bfloat16 or wider, within the bound.
A program may use at most 64 MiB of HBM per device.

v0:
```python
import jax
import jax.numpy as jnp
from jax import lax
from jax.sharding import PartitionSpec as P


def contract(left, right, left_dim, right_dim):
    return lax.dot_general(
        left, right, (((left_dim,), (right_dim,)), ((), ())), preferred_element_type=jnp.float32
    )


def rms_back(grad_rows, unit_rows, inv_rms, gain_rows):
    scaled = gain_rows * grad_rows
    inner = jnp.mean(scaled * unit_rows, axis=-1, keepdims=True)
    return inv_rms * (scaled - unit_rows * inner)


def on_device(tokens, grad_out, norm_gain, gate_weight, up_weight, down_weight):
    full_tokens, full_grad = (
        lax.all_gather(tokens, "tp", axis=1, tiled=True),
        lax.all_gather(grad_out, "tp", axis=1, tiled=True),
    )
    floated = full_tokens.astype(jnp.float32)
    inv_rms = lax.rsqrt(jnp.mean(floated * floated, axis=-1, keepdims=True) + 1e-06)
    unit_rows = floated * inv_rms
    gain_rows = norm_gain[None, :]
    normed = (unit_rows * gain_rows).astype(jnp.bfloat16)
    gate_full, up_full, down_full = (
        lax.all_gather(gate_weight, "fs", axis=1, tiled=True),
        lax.all_gather(up_weight, "fs", axis=1, tiled=True),
        lax.all_gather(down_weight, "fs", axis=1, tiled=True),
    )
    grad_hidden = 0.5 * contract(full_grad, down_full, 1, 1)
    factor = (full_tokens.shape[0] * lax.axis_size("fs")) ** (-0.5)
    gate_pre = contract(normed, gate_full, 1, 1)
    up_pre = contract(normed, up_full, 1, 1)
    sigma = jax.nn.sigmoid(gate_pre)
    active = gate_pre * sigma
    hidden = (active * up_pre).astype(jnp.bfloat16)
    term_down = 0.5 * factor * contract(hidden, full_grad, 0, 0)
    gate_grad_pre = (grad_hidden * up_pre * sigma * (1.0 + gate_pre * (1.0 - sigma))).astype(
        jnp.bfloat16
    )
    term_gate = factor * contract(gate_grad_pre, normed, 0, 0)
    up_grad_pre = (grad_hidden * active).astype(jnp.bfloat16)
    term_up = factor * contract(up_grad_pre, normed, 0, 0)
    grad_rows = jnp.dot(gate_grad_pre, gate_full, preferred_element_type=jnp.float32)
    grad_rows = grad_rows + jnp.dot(up_grad_pre, up_full, preferred_element_type=jnp.float32)
    partial_value = rms_back(grad_rows, unit_rows, inv_rms, gain_rows)
    summed = lax.psum_scatter(
        partial_value.astype(jnp.bfloat16), "tp", scatter_dimension=1, tiled=True
    ).astype(jnp.float32)
    grad_input = (grad_out.astype(jnp.float32) + summed).astype(jnp.bfloat16)
    grad_gate, grad_up, grad_down = (
        lax.psum_scatter(
            term_gate.astype(jnp.bfloat16), "fs", scatter_dimension=1, tiled=True
        ).astype(jnp.float32),
        lax.psum_scatter(
            term_up.astype(jnp.bfloat16), "fs", scatter_dimension=1, tiled=True
        ).astype(jnp.float32),
        lax.psum_scatter(
            term_down.astype(jnp.bfloat16), "fs", scatter_dimension=1, tiled=True
        ).astype(jnp.float32),
    )
    width_total = gate_weight.shape[1] * lax.axis_size("fs")
    gate_rows, up_rows, down_rows = lax.psum(
        (
            jnp.sum(grad_gate * grad_gate, axis=1),
            jnp.sum(grad_up * grad_up, axis=1),
            jnp.sum(grad_down * grad_down, axis=1),
        ),
        "fs",
    )
    row_squares = jnp.stack([gate_rows, up_rows, down_rows]) / width_total
    return (grad_input, grad_gate, grad_up, grad_down, row_squares)


def solution(mesh):
    in_specs = (P("fs", "tp"), P("fs", "tp"), P(), P("tp", "fs"), P("tp", "fs"), P("tp", "fs"))
    out_specs = (P("fs", "tp"), P("tp", "fs"), P("tp", "fs"), P("tp", "fs"), P(None, "tp"))
    return jax.shard_map(
        on_device, mesh=mesh, in_specs=in_specs, out_specs=out_specs, check_vma=False
    )
```

profile of v0, /device:TPU:0, one launch (start us, length us, event | category | flops | bytes accessed | tf_op | source)
XLA Modules:
  0.0 560.3 jit_solution(2466736034148901579)
XLA Ops:
  7.2 0.0 copy-start.4
  7.2 0.0 all-gather.6.cloned.1.call-start
  7.2 0.7 all-gather.6.cloned.1.call-update
  7.9 0.0 all-gather.14.cloned.1.call-start
  8.0 0.7 all-gather.14.cloned.1.call-update
  8.7 0.0 all-gather.12.cloned.1.call-start
  8.7 0.7 all-gather.12.cloned.1.call-update
  9.4 0.0 all-gather.8.cloned.1.call-start
  9.4 0.5 all-gather.8.cloned.1.call-update
  10.0 0.0 all-gather.10.cloned.1.call-start
  10.0 0.5 all-gather.10.cloned.1.call-update
  10.6 0.0 reduce-scatter.11.cloned.1.call-start
  10.6 36.2 %all-gather.6.cloned.1.call-done = bf16[1024,2048]{1,0:T(8,128)(2,1)} async-done(((bf16[1024,512]{1,0:T(8,128)(2,1)}), bf16[1024,2048]{1,0:T(8,128)(2,1)}) %all-gather.6.cloned.1.call-update) | async-done | bytes 4194320 | tf_op jit(solution)/shard_map/all_gather | solution.py:21
  46.8 3.1 fusion.8
  49.8 61.6 %all-gather.14.cloned.1.call-done = bf16[768,2048]{1,0:T(8,128)(2,1)} async-done(((bf16[768,256]{1,0:T(8,128)(2,1)}), bf16[768,2048]{1,0:T(8,128)(2,1)}) %all-gather.14.cloned.1.call-update) | async-done | bytes 3145744 | tf_op jit(solution)/shard_map/all_gather | solution.py:30
  111.5 0.0 copy-done.4
  111.5 8.3 %fusion.14 = f32[1024,768]{1,0:T(8,128)} fusion(bf16[768,2048]{1,0:T(8,128)(2,1)} %all-gather.14.cloned.1.call-done, bf16[1024,2048]{1,0:T(8,128)(2,1)} %all-gather.6.cloned.1.call-done, f32[2048]{0:T(1024)S(1)} %copy-done.4, f32[1024]{0:T(1024)S(1)} %add_rsqrt_fusion), kind=kOutput, calls=%fused_computation.28 | convolution fusion | flops 3229614080 | bytes 10498048 | tf_op jit(solution)/shard_map/dot_general | solution.py:8
  119.8 54.6 %all-gather.12.cloned.1.call-done = bf16[768,2048]{1,0:T(8,128)(2,1)} async-done(((bf16[768,256]{1,0:T(8,128)(2,1)}), bf16[768,2048]{1,0:T(8,128)(2,1)}) %all-gather.12.cloned.1.call-update) | async-done | bytes 3145744 | tf_op jit(solution)/shard_map/all_gather | solution.py:31
  174.4 8.4 %fusion.16 = f32[1024,768]{1,0:T(8,128)} fusion(bf16[768,2048]{1,0:T(8,128)(2,1)} %all-gather.12.cloned.1.call-done, bf16[1024,2048]{1,0:T(8,128)(2,1)} %all-gather.6.cloned.1.call-done, f32[2048]{0:T(1024)S(1)} %copy-done.4, f32[1024]{0:T(1024)S(1)} %add_rsqrt_fusion), kind=kOutput, calls=%fused_computation.29 | convolution fusion | flops 3229614080 | bytes 10498048 | tf_op jit(solution)/shard_map/dot_general | solution.py:8
  182.8 25.7 %all-gather.8.cloned.1.call-done = bf16[1024,2048]{1,0:T(8,128)(2,1)} async-done(((bf16[1024,512]{1,0:T(8,128)(2,1)}), bf16[1024,2048]{1,0:T(8,128)(2,1)}) %all-gather.8.cloned.1.call-update) | async-done | bytes 4194320 | tf_op jit(solution)/shard_map/all_gather | solution.py:22
  208.5 9.2 %multiply_convert_fusion = bf16[768,2048]{1,0:T(8,128)(2,1)} fusion(bf16[1024,2048]{1,0:T(8,128)(2,1)} %all-gather.8.cloned.1.call-done, f32[1024,768]{1,0:T(8,128)} %fusion.16, f32[1024,768]{1,0:T(8,128)} %fusion.14), kind=kOutput, calls=%fused_computation.12 | convolution fusion | flops 3229089792 | bytes 13631488 | tf_op jit(solution)/shard_map/dot_general | solution.py:8
  217.7 0.0 reduce-scatter.11.cloned.1.call-update
  217.8 0.2 reduce-scatter.9.cloned.1.call-start
  218.0 55.1 %all-gather.10.cloned.1.call-done = bf16[768,2048]{1,0:T(8,128)(2,1)} async-done(((bf16[768,256]{1,0:T(8,128)(2,1)}), bf16[768,2048]{1,0:T(8,128)(2,1)}) %all-gather.10.cloned.1.call-update) | async-done | bytes 3145744 | tf_op jit(solution)/shard_map/all_gather | solution.py:32
  273.1 0.0 copy-start
  273.1 9.4 %multiply_convert_fusion.4 = (bf16[1024,768]{1,0:T(8,128)(2,1)S(1)}, bf16[1024,768]{1,0:T(8,128)(2,1)S(1)}) fusion(f32[1024,768]{1,0:T(8,128)} %fusion.14, f32[1024,768]{1,0:T(8,128)} %fusion.16, bf16[1024,2048]{1,0:T(8,128)(2,1)} %all-gather.8.cloned.1.call-done, bf16[768,2048]{1,0:T(8,128)(2,1)} %all-gather.10.cloned.1.call-done), kind=kOutput, calls=%fused_computation.16 | convolution fusion | flops 3232235520 | bytes 16777216 | tf_op jit(solution)/shard_map/dot_general | solution.py:8
  282.5 0.0 copy-done
  282.5 5.3 multiply_convert_fusion.1
  287.7 0.0 reduce-scatter.9.cloned.1.call-update
  287.8 0.0 reduce-scatter.7.cloned.1.call-start
  287.8 7.5 %multiply_convert_fusion.2 = bf16[768,2048]{1,0:T(8,128)(2,1)} fusion(bf16[1024,768]{1,0:T(8,128)(2,1)S(1)} %get-tuple-element.15, bf16[1024,2048]{1,0:T(8,128)(2,1)} %all-gather.6.cloned.1.call-done, f32[2048]{0:T(1024)S(1)} %copy-done.4, f32[1024]{0:T(1024)S(1)} %add_rsqrt_fusion), kind=kOutput, calls=%fused_computation.14 | convolution fusion | flops 3232759808 | bytes 8925184 | tf_op jit(solution)/shard_map/dot_general | solution.py:8
  295.3 0.0 reduce-scatter.7.cloned.1.call-update
  295.3 0.3 reduce-scatter.5.cloned.1.call-start
  295.6 0.0 copy-start.1
  295.6 0.0 copy-start.3
  295.6 5.6 fusion.18
  301.2 0.0 copy-done.1
  301.2 0.0 copy-done.3
  301.2 4.1 fusion.4
  305.3 3.1 fusion.7
  308.4 0.0 copy-start.2
  308.4 0.0 reduce-scatter.5.cloned.1.call-update
  308.4 41.2 %reduce-scatter.11.cloned.1.call-done = bf16[768,256]{1,0:T(8,128)(2,1)} async-done(((bf16[768,2048]{1,0:T(8,128)(2,1)}), bf16[768,256]{1,0:T(8,128)(2,1)}) %reduce-scatter.11.cloned.1.call-update) | async-done | bytes 393232 | tf_op jit(solution)/shard_map/reduce_scatter | solution.py:62
  349.6 1.9 multiply_reduce_fusion
  351.6 75.8 %reduce-scatter.9.cloned.1.call-done = bf16[768,256]{1,0:T(8,128)(2,1)} async-done(((bf16[768,2048]{1,0:T(8,128)(2,1)}), bf16[768,256]{1,0:T(8,128)(2,1)}) %reduce-scatter.9.cloned.1.call-update) | async-done | bytes 393232 | tf_op jit(solution)/shard_map/reduce_scatter | solution.py:59
  427.4 1.9 multiply_reduce_fusion.1
  429.4 75.8 %reduce-scatter.7.cloned.1.call-done = bf16[768,256]{1,0:T(8,128)(2,1)} async-done(((bf16[768,2048]{1,0:T(8,128)(2,1)}), bf16[768,256]{1,0:T(8,128)(2,1)}) %reduce-scatter.7.cloned.1.call-update) | async-done | bytes 393232 | tf_op jit(solution)/shard_map/reduce_scatter | solution.py:56
  505.2 1.9 multiply_reduce_fusion.2
  507.1 20.0 %all-reduce = (f32[1,768]{1,0:T(1,128)S(1)}, f32[1,768]{1,0:T(1,128)S(1)}, f32[1,768]{1,0:T(1,128)S(1)}) all-reduce(f32[1,768]{1,0:T(1,128)S(1)} %stack.14, f32[1,768]{1,0:T(1,128)S(1)} %stack.13, f32[1,768]{1,0:T(1,128)S(1)} %stack.12), channel_id=1, replica_groups=mesh['fs'=8,'tp'=4] {'fs'}, use_global_device_ids=true, to_apply=%region_11.0 | all-reduce | flops 2304 | bytes 18432 | tf_op jit(solution)/shard_map/psum | solution.py:67
  527.1 0.6 maximum_multiply_fusion
  527.7 23.5 %reduce-scatter.5.cloned.1.call-done = bf16[1024,512]{1,0:T(8,128)(2,1)} async-done(((bf16[1024,2048]{1,0:T(8,128)(2,1)}), bf16[1024,512]{1,0:T(8,128)(2,1)}) %reduce-scatter.5.cloned.1.call-update) | async-done | bytes 1048592 | tf_op jit(solution)/shard_map/reduce_scatter | solution.py:51
  551.2 0.0 copy-done.2
  551.2 2.5 add_convert_fusion
  (5 shorter events, 0.0 us)
Async XLA Ops:
  7.2 104.3 %copy-start.4 = (f32[2048]{0:T(1024)S(1)}, f32[2048]{0:T(1024)}, u32[]{:S(2)}) copy-start(f32[2048]{0:T(1024)} %param.8) | copy-start | bytes 24580
  7.2 39.6 %all-gather.6.cloned.1.call-start = ((), (), s32[]{:S(2)}) async-start(), calls=%async_computation.4 | async-start | bytes 5242880 | tf_op jit(solution)/shard_map/all_gather | solution.py:21
  7.9 103.6 %all-gather.14.cloned.1.call-start = ((), (), s32[]{:S(2)}) async-start(), calls=%async_computation.8 | async-start | bytes 3538944 | tf_op jit(solution)/shard_map/all_gather | solution.py:30
  8.7 165.7 %all-gather.12.cloned.1.call-start = ((), (), s32[]{:S(2)}) async-start(), calls=%async_computation.7 | async-start | bytes 3538944 | tf_op jit(solution)/shard_map/all_gather | solution.py:31
  9.4 199.1 %all-gather.8.cloned.1.call-start = ((), (), s32[]{:S(2)}) async-start(), calls=%async_computation.5 | async-start | bytes 5242880 | tf_op jit(solution)/shard_map/all_gather | solution.py:22
  10.0 263.1 %all-gather.10.cloned.1.call-start = ((), (), s32[]{:S(2)}) async-start(), calls=%async_computation.6 | async-start | bytes 3538944 | tf_op jit(solution)/shard_map/all_gather | solution.py:32
  10.6 339.1 %reduce-scatter.11.cloned.1.call-start = ((), (), s32[]{:S(2)}) async-start(), calls=%async_computation.12 | async-start | bytes 3538944 | tf_op jit(solution)/shard_map/reduce_scatter | solution.py:62
  217.8 209.6 %reduce-scatter.9.cloned.1.call-start = ((), (), s32[]{:S(2)}) async-start(), calls=%async_computation.11 | async-start | bytes 3538944 | tf_op jit(solution)/shard_map/reduce_scatter | solution.py:59
  273.1 9.4 %copy-start = (bf16[1024,2048]{1,0:T(8,128)(2,1)S(1)}, bf16[1024,2048]{1,0:T(8,128)(2,1)}, u32[]{:S(2)}) copy-start(bf16[1024,2048]{1,0:T(8,128)(2,1)} %all-gather.6.cloned.1.call-done) | copy-start | bytes 12582916
  287.8 217.4 %reduce-scatter.7.cloned.1.call-start = ((), (), s32[]{:S(2)}) async-start(), calls=%async_computation.10 | async-start | bytes 3538944 | tf_op jit(solution)/shard_map/reduce_scatter | solution.py:56
  295.3 255.9 %reduce-scatter.5.cloned.1.call-start = ((), (), s32[]{:S(2)}) async-start(), calls=%async_computation.9 | async-start | bytes 5242880 | tf_op jit(solution)/shard_map/reduce_scatter | solution.py:51
  295.6 5.6 copy-start.1
  295.6 5.6 copy-start.3
  308.4 242.8 %copy-start.2 = (bf16[1024,512]{1,0:T(8,128)(2,1)S(1)}, bf16[1024,512]{1,0:T(8,128)(2,1)}, u32[]{:S(2)}) copy-start(bf16[1024,512]{1,0:T(8,128)(2,1)} %param.7) | copy-start | bytes 3145732
Sparse Core Ops, SparseCore 0:
  9.5 37.1 all-gather.5
  48.8 62.6 all-gather.13
  113.5 60.8 all-gather.11
  175.8 32.6 all-gather.7
  210.4 62.6 all-gather.9
  276.5 73.0 reduce-scatter.10
  353.2 74.1 reduce-scatter.8
  431.0 74.1 reduce-scatter.6
  507.7 43.4 reduce-scatter.4
where the time goes:
time: 561 us; the launch traced here: 560 us
  waiting for transfers between devices  453 us (81%)
  matrix products  57.7 us (10%)
  blocking collectives  20 us (4%)
  other arithmetic  15.1 us (3%)
  between operations  13.9 us (2%)
    reduce_scatter x1, waiting for transfers between devices, on_device(): lax.psum_scatter(term_up.astype(jnp.bfloat16), 'fs', scatter_dimension=1,...  75.8 us
    reduce_scatter x1, waiting for transfers between devices, on_device(): lax.psum_scatter(term_gate.astype(jnp.bfloat16), 'fs', scatter_dimension=...  75.8 us
    all_gather x1, waiting for transfers between devices, on_device(): lax.all_gather(gate_weight, 'fs', axis=1, tiled=True)  61.6 us
    all_gather x1, waiting for transfers between devices, on_device(): lax.all_gather(down_weight, 'fs', axis=1, tiled=True)  55.1 us
    all_gather x1, waiting for transfers between devices, on_device(): lax.all_gather(up_weight, 'fs', axis=1, tiled=True)  54.6 us
    dot_general x6, matrix products, contract(): lax.dot_general(left, right, (((left_dim,), (right_dim,)), ((), ())), pre...  48.1 us
    reduce_scatter x1, waiting for transfers between devices, on_device(): lax.psum_scatter(term_down.astype(jnp.bfloat16), 'fs', scatter_dimension=...  41.2 us
    all_gather x1, waiting for transfers between devices, on_device(): lax.all_gather(tokens, 'tp', axis=1, tiled=True)  36.2 us
  transfers between devices with their start and end apart: 9, of which 9 were waited for; matrix products, arithmetic and copies ran while one was open for 13% of the time, Pallas kernels for 0%

commit v1 on v0

v1 whole, which is shorter than its diff:
```python
import functools
import math

import jax
import jax.numpy as jnp
from jax import lax
from jax.experimental import pallas as pl
from jax.experimental.pallas import tpu as pltpu
from jax.sharding import PartitionSpec as P

MESH = pl.DeviceIdType.MESH
ANY = pl.BlockSpec(memory_space=pl.ANY)
VMEM = pl.BlockSpec(memory_space=pltpu.VMEM)


def contract(left, right, left_dim, right_dim):
    return lax.dot_general(
        left, right, (((left_dim,), (right_dim,)), ((), ())), preferred_element_type=jnp.float32
    )


def rms_back(grad_rows, unit_rows, inv_rms, gain_rows):
    scaled = gain_rows * grad_rows
    inner = jnp.mean(scaled * unit_rows, axis=-1, keepdims=True)
    return inv_rms * (scaled - unit_rows * inner)


def axes_of(n_fs, n_tp):
    nx = max(1, math.isqrt(max(1, n_fs // 2)))
    while n_fs % nx:
        nx -= 1
    nc = 2 if n_tp % 2 == 0 else 1
    return n_fs // nx, nx, n_tp // nc, nc


def greet(targets):
    barrier = pltpu.get_barrier_semaphore()
    for target in targets:
        pl.semaphore_signal(barrier, inc=1, device_id=target, device_id_type=MESH)
    pl.semaphore_wait(barrier, len(targets))


def remote(src, dst, send_sem, recv_sem, target):
    return pltpu.make_async_remote_copy(
        src_ref=src, dst_ref=dst, send_sem=send_sem, recv_sem=recv_sem,
        device_id=target, device_id_type=MESH,
    )


def block_of(ref, index, width):
    if len(ref.shape) == 3:
        return ref.at[index]
    return ref.at[:, pl.ds(pl.multiple_of(index * width, 128), width)]


def gather_kernel(dims, *refs):
    nz, nx, ny, nc = dims
    small, full, held = refs[:5], refs[5:10], refs[10:15]
    out_sem, in_sem, zs, zr, xs, xr, ys, yr, cs, cr = refs[15:]
    fs, tp = lax.axis_index("fs"), lax.axis_index("tp")
    z, x, y, c = fs // nx, fs % nx, tp // nc, tp % nc

    def z_dev(r):
        return {"fs": lax.rem(z + r, nz) * nx + x}

    def x_dev(q):
        return {"fs": z * nx + lax.rem(x + q, nx)}

    def y_dev(r):
        return {"tp": lax.rem(y + r, ny) * nc + c}

    def c_dev(q):
        return {"tp": y * nc + lax.rem(c + q, nc)}

    greet(
        [z_dev(r) for r in range(1, nz)] + [x_dev(q) for q in range(1, nx)]
        + [y_dev(r) for r in range(1, ny)] + [c_dev(q) for q in range(1, nc)]
    )
    width = [ref.shape[1] for ref in small]
    sends = []

    def go(copy):
        copy.start()
        sends.append(copy)

    acts, mats = (0, 1), (2, 3, 4)
    for a in acts:
        for r in range(1, ny):
            go(remote(small[a], block_of(full[a], tp, width[a]), ys.at[a, r], yr.at[a, r], y_dev(r)))
    z_order = [r for r in range(2, nz)] + [1] if nz > 1 else []
    for m in mats:
        for r in z_order:
            go(remote(small[m], block_of(full[m], fs, width[m]), zs.at[m - 2, r], zr.at[m - 2, r], z_dev(r)))
        for q in range(1, nx):
            go(remote(small[m], block_of(full[m], fs, width[m]), xs.at[m - 2, 0, q], xr.at[m - 2, 0, q], x_dev(q)))
    for a in acts:
        for q in range(1, nc):
            go(remote(small[a], block_of(full[a], tp, width[a]), cs.at[a, 0, q], cr.at[a, 0, q], c_dev(q)))
    loads = [pltpu.make_async_copy(small[i], held[i], in_sem.at[i]) for i in range(5)]
    for load in loads:
        load.start()
    stores = []
    for i in range(5):
        loads[i].wait()
        index = tp if i < 2 else fs
        stores.append(pltpu.make_async_copy(held[i], block_of(full[i], index, width[i]), out_sem.at[i]))
        stores[i].start()

    def from_y(a, r):
        origin = lax.rem(y + ny - r, ny) * nc + c
        block = block_of(full[a], origin, width[a])
        remote(block, block, ys.at[a, r], yr.at[a, r], y_dev(r)).wait_recv()
        for q in range(1, nc):
            go(remote(block, block, cs.at[a, r, q], cr.at[a, r, q], c_dev(q)))

    def from_z(m, r):
        origin = lax.rem(z + nz - r, nz) * nx + x
        block = block_of(full[m], origin, width[m])
        remote(block, block, zs.at[m - 2, r], zr.at[m - 2, r], z_dev(r)).wait_recv()
        for q in range(1, nx):
            go(remote(block, block, xs.at[m - 2, r, q], xr.at[m - 2, r, q], x_dev(q)))

    late = [(a, r) for a in acts for r in range(1, ny)]
    for m in mats:
        for r in z_order:
            from_z(m, r)
        if late:
            from_y(*late.pop(0))
    for a, r in late:
        from_y(a, r)
    for m in mats:
        for r in range(nz):
            for q in range(1, nx):
                origin = lax.rem(z + nz - r, nz) * nx + lax.rem(x + nx - q, nx)
                block = block_of(full[m], origin, width[m])
                remote(block, block, xs.at[m - 2, r, q], xr.at[m - 2, r, q], x_dev(q)).wait_recv()
    for a in acts:
        for r in range(ny):
            for q in range(1, nc):
                origin = lax.rem(y + ny - r, ny) * nc + lax.rem(c + nc - q, nc)
                block = block_of(full[a], origin, width[a])
                remote(block, block, cs.at[a, r, q], cr.at[a, r, q], c_dev(q)).wait_recv()
    for store in stores:
        store.wait()
    for copy in sends:
        copy.wait_send()


def gather_all(dims, arrays):
    nz, nx, ny, nc = dims
    shapes = []
    for i, a in enumerate(arrays):
        n = ny * nc if i < 2 else nz * nx
        rows, cols = a.shape
        shape = (rows, n * cols) if cols % 128 == 0 else (n, rows, cols)
        shapes.append(jax.ShapeDtypeStruct(shape, a.dtype))
    dma = pltpu.SemaphoreType.DMA
    full = pl.pallas_call(
        functools.partial(gather_kernel, dims),
        out_shape=shapes,
        in_specs=[ANY] * 5,
        out_specs=[ANY] * 5,
        scratch_shapes=[pltpu.VMEM(a.shape, a.dtype) for a in arrays]
        + [
            dma((5,)), dma((5,)), dma((3, nz)), dma((3, nz)), dma((3, nz, nx)), dma((3, nz, nx)),
            dma((2, ny)), dma((2, ny)), dma((2, ny, nc)), dma((2, ny, nc)),
        ],
        compiler_params=pltpu.CompilerParams(collective_id=0, has_side_effects=True),
        name="gather",
    )(*arrays)
    return [
        a if a.ndim == 2 else jnp.swapaxes(a, 0, 1).reshape(a.shape[1], -1) for a in full
    ]


def reduce_kernel(dims, width_total, *refs):
    nz, nx, ny, nc = dims
    terms, part, grad = refs[:3], refs[3], refs[4]
    outs, out_x, out_sq = refs[5:8], refs[8], refs[9]
    (own, x_in, z_out, z_in, p_own, c_in, y_out, y_in, sq_out, sq_in,
     own_sem, p_sem, xs, xr, zs, zr, cs, cr, ys, yr, qs, qr) = refs[10:]
    n_fs = nz * nx
    fs, tp = lax.axis_index("fs"), lax.axis_index("tp")
    z, x, y, c = fs // nx, fs % nx, tp // nc, tp % nc
    width, cols = outs[0].shape[1], out_x.shape[1]
    f32, bf16 = jnp.float32, jnp.bfloat16

    def z_index(r):
        return lax.rem(z + r, nz) * nx + x

    def fs_dev(k):
        return {"fs": lax.rem(fs + k, n_fs)}

    def x_dev(q):
        return {"fs": z * nx + lax.rem(x + q, nx)}

    def y_dev(r):
        return {"tp": lax.rem(y + r, ny) * nc + c}

    def c_dev(q):
        return {"tp": y * nc + lax.rem(c + q, nc)}

    greet(
        [fs_dev(k) for k in range(1, n_fs)]
        + [y_dev(r) for r in range(1, ny)] + [c_dev(q) for q in range(1, nc)]
    )
    sends = []

    def go(copy):
        copy.start()
        sends.append(copy)

    z_order = ([r for r in range(2, nz)] + [1] if nz > 1 else []) + [0]
    y_order = [r for r in range(1, ny)] + [0]
    for r in y_order:
        for q in range(1, nc):
            index = lax.rem(y + r, ny) * nc + lax.rem(c + q, nc)
            go(remote(block_of(part, index, cols), c_in.at[r, q - 1], cs.at[r, q], cr.at[r, q], c_dev(q)))
    for r in z_order:
        for w in range(3):
            for q in range(1, nx):
                index = lax.rem(z + r, nz) * nx + lax.rem(x + q, nx)
                go(remote(block_of(terms[w], index, width), x_in.at[w, r, q - 1], xs.at[w, r, q], xr.at[w, r, q], x_dev(q)))
    p_loads = {}
    for r in y_order:
        index = lax.rem(y + r, ny) * nc + c
        p_loads[r] = pltpu.make_async_copy(block_of(part, index, cols), p_own.at[r], p_sem.at[r])
        p_loads[r].start()
    loads = {}
    for r in z_order:
        for w in range(3):
            loads[w, r] = pltpu.make_async_copy(block_of(terms[w], z_index(r), width), own.at[w, r], own_sem.at[w, r])
            loads[w, r].start()

    def pair_wait(r):
        p_loads[r].wait()
        for q in range(1, nc):
            remote(p_own.at[r], c_in.at[r, q - 1], cs.at[r, q], cr.at[r, q], c_dev(q)).wait_recv()

    def wide_wait(w, r):
        loads[w, r].wait()
        for q in range(1, nx):
            remote(own.at[w, r], x_in.at[w, r, q - 1], xs.at[w, r, q], xr.at[w, r, q], x_dev(q)).wait_recv()

    def tiles(rows, body):
        step = math.gcd(rows, 128)

        def run(i, carry):
            body(pl.ds(pl.multiple_of(i * step, step), step))
            return carry

        lax.fori_loop(0, rows // step, run, 0)

    n_rows, n_hid = out_x.shape[0], outs[0].shape[0]
    for r in range(1, ny):
        pair_wait(r)

        def add_pair(rows):
            acc = p_own[r, rows, :].astype(f32)
            for q in range(1, nc):
                acc = acc + c_in[r, q - 1, rows, :].astype(f32)
            y_out[r, rows, :] = acc.astype(bf16)

        tiles(n_rows, add_pair)
        go(remote(y_out.at[r], y_in.at[r], ys.at[r], yr.at[r], y_dev(r)))
    for r in z_order[:-1]:
        for w in range(3):
            wide_wait(w, r)

            def add_wide(rows):
                acc = own[w, r, rows, :].astype(f32)
                for q in range(1, nx):
                    acc = acc + x_in[w, r, q - 1, rows, :].astype(f32)
                z_out[w, r, rows, :] = acc.astype(bf16)

            tiles(n_hid, add_wide)
            go(remote(z_out.at[w, r], z_in.at[w, r], zs.at[w, r], zr.at[w, r], {"fs": z_index(r)}))
    pair_wait(0)
    for r in range(1, ny):
        remote(y_out.at[r], y_in.at[r], ys.at[r], yr.at[r], y_dev(r)).wait_recv()

    def finish_rows(rows):
        acc = grad[rows, :].astype(f32) + p_own[0, rows, :].astype(f32)
        for q in range(1, nc):
            acc = acc + c_in[0, q - 1, rows, :].astype(f32)
        for r in range(1, ny):
            acc = acc + y_in[r, rows, :].astype(f32)
        out_x[rows, :] = acc.astype(bf16)

    tiles(n_rows, finish_rows)
    ones = jnp.ones((8, width), f32)
    for w in range(3):
        wide_wait(w, 0)
        for r in z_order[:-1]:
            remote(z_out.at[w, r], z_in.at[w, r], zs.at[w, r], zr.at[w, r], {"fs": z_index(r)}).wait_recv()

        def finish_term(rows):
            acc = own[w, 0, rows, :].astype(f32)
            for q in range(1, nx):
                acc = acc + x_in[w, 0, q - 1, rows, :].astype(f32)
            for r in z_order[:-1]:
                acc = acc + z_in[w, r, rows, :].astype(f32)
            outs[w][rows, :] = acc
            squares = lax.dot_general(
                ones, acc * acc, (((1,), (1,)), ((), ())),
                precision=lax.Precision.HIGHEST, preferred_element_type=f32,
            )
            sq_out[pl.ds(w, 1), rows] = squares[:1]

        tiles(n_hid, finish_term)
    for k in range(1, n_fs):
        go(remote(sq_out, sq_in.at[k], qs.at[k], qr.at[k], fs_dev(k)))
    total = sq_out[...]
    for k in range(1, n_fs):
        remote(sq_out, sq_in.at[k], qs.at[k], qr.at[k], fs_dev(k)).wait_recv()
        total = total + sq_in[k]
    out_sq[...] = total / width_total
    for copy in sends:
        copy.wait_send()


def reduce_all(dims, terms, part, grad_out, width):
    nz, nx, ny, nc = dims
    n_fs = nz * nx
    hid = terms[0].shape[0]
    rows, cols = grad_out.shape
    if width % 128:
        terms = [jnp.swapaxes(t.reshape(hid, n_fs, width), 0, 1) for t in terms]
    dma, bf16, f32 = pltpu.SemaphoreType.DMA, jnp.bfloat16, jnp.float32
    return pl.pallas_call(
        functools.partial(reduce_kernel, dims, n_fs * width),
        out_shape=[jax.ShapeDtypeStruct((hid, width), f32)] * 3
        + [jax.ShapeDtypeStruct((rows, cols), bf16), jax.ShapeDtypeStruct((3, hid), f32)],
        in_specs=[ANY] * 4 + [VMEM],
        out_specs=[VMEM] * 5,
        scratch_shapes=[
            pltpu.VMEM((3, nz, hid, width), bf16),
            pltpu.VMEM((3, nz, max(1, nx - 1), hid, width), bf16),
            pltpu.VMEM((3, nz, hid, width), bf16),
            pltpu.VMEM((3, nz, hid, width), bf16),
            pltpu.VMEM((ny, rows, cols), bf16),
            pltpu.VMEM((ny, max(1, nc - 1), rows, cols), bf16),
            pltpu.VMEM((ny, rows, cols), bf16),
            pltpu.VMEM((ny, rows, cols), bf16),
            pltpu.VMEM((3, hid), f32),
            pltpu.VMEM((n_fs, 3, hid), f32),
            dma((3, nz)), dma((ny,)),
            dma((3, nz, nx)), dma((3, nz, nx)), dma((3, nz)), dma((3, nz)),
            dma((ny, nc)), dma((ny, nc)), dma((ny,)), dma((ny,)),
            dma((n_fs,)), dma((n_fs,)),
        ],
        compiler_params=pltpu.CompilerParams(
            collective_id=1, has_side_effects=True, vmem_limit_bytes=60 * 2**20
        ),
        name="reduce",
    )(*terms, part, grad_out)


def on_device(dims, tokens, grad_out, norm_gain, gate_weight, up_weight, down_weight):
    full_tokens, full_grad, gate_full, up_full, down_full = gather_all(
        dims, (tokens, grad_out, gate_weight, up_weight, down_weight)
    )
    floated = full_tokens.astype(jnp.float32)
    inv_rms = lax.rsqrt(jnp.mean(floated * floated, axis=-1, keepdims=True) + 1e-06)
    unit_rows = floated * inv_rms
    gain_rows = norm_gain[None, :]
    normed = (unit_rows * gain_rows).astype(jnp.bfloat16)
    grad_hidden = 0.5 * contract(full_grad, down_full, 1, 1)
    factor = (full_tokens.shape[0] * lax.axis_size("fs")) ** (-0.5)
    gate_pre = contract(normed, gate_full, 1, 1)
    up_pre = contract(normed, up_full, 1, 1)
    sigma = jax.nn.sigmoid(gate_pre)
    active = gate_pre * sigma
    hidden = (active * up_pre).astype(jnp.bfloat16)
    term_down = 0.5 * factor * contract(hidden, full_grad, 0, 0)
    gate_grad_pre = (grad_hidden * up_pre * sigma * (1.0 + gate_pre * (1.0 - sigma))).astype(
        jnp.bfloat16
    )
    term_gate = factor * contract(gate_grad_pre, normed, 0, 0)
    up_grad_pre = (grad_hidden * active).astype(jnp.bfloat16)
    term_up = factor * contract(up_grad_pre, normed, 0, 0)
    grad_rows = jnp.dot(gate_grad_pre, gate_full, preferred_element_type=jnp.float32)
    grad_rows = grad_rows + jnp.dot(up_grad_pre, up_full, preferred_element_type=jnp.float32)
    partial_value = rms_back(grad_rows, unit_rows, inv_rms, gain_rows).astype(jnp.bfloat16)
    terms = [t.astype(jnp.bfloat16) for t in (term_gate, term_up, term_down)]
    grad_gate, grad_up, grad_down, grad_input, row_squares = reduce_all(
        dims, terms, partial_value, grad_out, gate_weight.shape[1]
    )
    return (grad_input, grad_gate, grad_up, grad_down, row_squares)


def solution(mesh):
    in_specs = (P("fs", "tp"), P("fs", "tp"), P(), P("tp", "fs"), P("tp", "fs"), P("tp", "fs"))
    out_specs = (P("fs", "tp"), P("tp", "fs"), P("tp", "fs"), P("tp", "fs"), P(None, "tp"))
    dims = axes_of(mesh.shape["fs"], mesh.shape["tp"])
    return jax.shard_map(
        functools.partial(on_device, dims), mesh=mesh, in_specs=in_specs, out_specs=out_specs,
        check_vma=False,
    )
```

time: 561 us -> 308 us (0.55)
  waiting for transfers between devices: 453 us -> 0 us
  Pallas kernels: 0 us -> 257 us
  matrix products: 57.7 us -> 37 us
  blocking collectives: 20 us -> 0 us
  between operations: 13.9 us -> 0.77 us
  other arithmetic: 15.1 us -> 6.44 us
  local copies, waits for them, and re-layouts: 0.03 us -> 7.03 us
    pallas_call x0 -> x2, Pallas kernels: none -> 257 us  [the longest x1 130 us: reduce_all(): pl.pallas_call(functools.partial(reduce_kernel, dims, n_fs * width), out_...]
    all_gather x5 -> x0, waiting for transfers between devices: 233 us -> none  [the longest x1 61.6 us: on_device(): lax.all_gather(gate_weight, 'fs', axis=1, tiled=True)]
    reduce_scatter x4 -> x0, waiting for transfers between devices: 216 us -> none  [the longest x1 75.8 us: on_device(): lax.psum_scatter(term_up.astype(jnp.bfloat16), 'fs', scatter_dimension=1,...]
    psum x1 -> x0, blocking collectives: 20 us -> none  [on_device(): lax.psum((jnp.sum(grad_gate * grad_gate, axis=1), jnp.sum(grad_up * grad_...]
    dot_general x6, matrix products: 48.1 us -> 29.6 us  [contract(): lax.dot_general(left, right, (((left_dim,), (right_dim,)), ((), ())), pre...]
    unnamed x10 -> x23, local copies, waits for them, and re-layouts: 0.02 us -> 7.03 us
    reduce_sum x3 -> x0, other arithmetic: 5.82 us -> none  [the longest x1 1.94 us: on_device(): jnp.sum(grad_down * grad_down, axis=1)]
  transfers between devices with their start and end apart: 9 -> 0, of which waited for: 9 -> 0; matrix products, arithmetic and copies ran while one was open for 13% -> 0% of each run, Pallas kernels for 0% -> 0%
where the time goes in v1:
time: 308 us
  Pallas kernels  257 us (83%)
  matrix products  37 us (12%)
  local copies, waits for them, and re-layouts  7.03 us (2%)
  other arithmetic  6.44 us (2%)
    pallas_call x1, Pallas kernels, reduce_all(): pl.pallas_call(functools.partial(reduce_kernel, dims, n_fs * width), out_...  130 us
    pallas_call x1, Pallas kernels, gather_all(): pl.pallas_call(functools.partial(gather_kernel, dims), out_shape=shapes,...  127 us
    dot_general x6, matrix products, contract(): lax.dot_general(left, right, (((left_dim,), (right_dim,)), ((), ())), pre...  29.6 us
    unnamed x23, local copies, waits for them, and re-layouts  7.03 us

profile of v1, /device:TPU:0, one launch (start us, length us, event | category | flops | bytes accessed | tf_op | source)
XLA Modules:
  0.0 307.9 jit_solution(697777022938474542)
XLA Ops:
  0.6 0.0 copy-start.4
  0.6 127.2 %gather.1 = (bf16[1024,2048]{1,0:T(8,128)(2,1)}, bf16[1024,2048]{1,0:T(8,128)(2,1)}, bf16[768,2048]{1,0:T(8,128)(2,1)}, bf16[768,2048]{1,0:T(8,128)(2,1)}, bf16[768,2048]{1,0:T(8,128)(2,1)}) custom-call(bf16[1024,512]{1,0:T(8,128)(2,1)} %refs_0_.1, bf16[1024,512]{1,0:T(8,128)(2,1)} %refs_4_.3, bf16[768,256]{1,0:T(8,128)(2,1)} %refs_2_.1, ...), custom_call_target="tpu_custom_call" | custom-call | tf_op jit(solution)/shard_map/gather/pallas_call | solution.py:158
  127.8 0.0 copy-start
  127.8 3.2 %fusion.8 = f32[1024]{0:T(1024)S(1)} fusion(bf16[1024,2048]{1,0:T(8,128)(2,1)} %get-tuple-element.17), kind=kLoop, calls=%fused_computation.10 | loop fusion | flops 6290432 | bytes 4198400 | tf_op jit(solution)/shard_map/reduce_sum | solution.py:364
  131.1 0.0 copy-done.4
  131.1 0.2 copy-done
  131.3 0.0 copy-start.1
  131.3 5.6 %fusion.14 = f32[1024,768]{1,0:T(8,128)S(1)} fusion(bf16[768,2048]{1,0:T(8,128)(2,1)} %get-tuple-element.19, bf16[1024,2048]{1,0:T(8,128)(2,1)S(1)} %copy-done, f32[2048]{0:T(1024)S(1)} %copy-done.4, f32[1024]{0:T(1024)S(1)} %add_rsqrt_fusion), kind=kOutput, calls=%fused_computation.23 | convolution fusion | flops 3229614080 | bytes 10498048 | tf_op jit(solution)/shard_map/dot_general | solution.py:17
  136.9 0.0 copy-done.1
  136.9 0.0 copy-start.6
  136.9 0.0 copy-start.8
  136.9 3.5 %fusion.16 = f32[1024,768]{1,0:T(8,128)S(1)} fusion(bf16[768,2048]{1,0:T(8,128)(2,1)S(1)} %copy-done.1, bf16[1024,2048]{1,0:T(8,128)(2,1)S(1)} %copy-done, f32[2048]{0:T(1024)S(1)} %copy-done.4, f32[1024]{0:T(1024)S(1)} %add_rsqrt_fusion), kind=kOutput, calls=%fused_computation.24 | convolution fusion | flops 3229614080 | bytes 10498048 | tf_op jit(solution)/shard_map/dot_general | solution.py:17
  140.4 0.0 copy-done.6
  140.4 0.0 copy-done.8
  140.4 4.4 %multiply_convert_fusion.4 = (bf16[1024,768]{1,0:T(8,128)(2,1)S(1)}, bf16[1024,768]{1,0:T(8,128)(2,1)S(1)}) fusion(f32[1024,768]{1,0:T(8,128)S(1)} %fusion.14, f32[1024,768]{1,0:T(8,128)S(1)} %fusion.16, bf16[1024,2048]{1,0:T(8,128)(2,1)S(1)} %copy-done.6, bf16[768,2048]{1,0:T(8,128)(2,1)S(1)} %copy-done.8), kind=kOutput, calls=%fused_computation.16 | convolution fusion | flops 3232235520 | bytes 16777216 | tf_op jit(solution)/shard_map/dot_general | solution.py:17
  144.8 5.4 %multiply_convert_fusion.refs_2_ = bf16[768,2048]{1,0:T(8,128)(2,1)} fusion(bf16[1024,2048]{1,0:T(8,128)(2,1)S(1)} %copy-done.6, f32[1024,768]{1,0:T(8,128)S(1)} %fusion.16, f32[1024,768]{1,0:T(8,128)S(1)} %fusion.14), kind=kOutput, calls=%fused_computation.12 | convolution fusion | flops 3229089792 | bytes 13631488 | tf_op jit(solution)/shard_map/dot_general | solution.py:17
  150.3 5.3 %multiply_convert_fusion.1.refs_1_ = bf16[768,2048]{1,0:T(8,128)(2,1)} fusion(bf16[1024,768]{1,0:T(8,128)(2,1)S(1)} %get-tuple-element.25, bf16[1024,2048]{1,0:T(8,128)(2,1)S(1)} %copy-done, f32[2048]{0:T(1024)S(1)} %copy-done.4, f32[1024]{0:T(1024)S(1)} %add_rsqrt_fusion), kind=kOutput, calls=%fused_computation.13 | convolution fusion | flops 3232759808 | bytes 8925184 | tf_op jit(solution)/shard_map/dot_general | solution.py:17
  155.6 0.0 copy-start.7
  155.6 5.3 %multiply_convert_fusion.2.refs_0_ = bf16[768,2048]{1,0:T(8,128)(2,1)} fusion(bf16[1024,768]{1,0:T(8,128)(2,1)S(1)} %get-tuple-element.26, bf16[1024,2048]{1,0:T(8,128)(2,1)S(1)} %copy-done, f32[2048]{0:T(1024)S(1)} %copy-done.4, f32[1024]{0:T(1024)S(1)} %add_rsqrt_fusion), kind=kOutput, calls=%fused_computation.14 | convolution fusion | flops 3232759808 | bytes 8925184 | tf_op jit(solution)/shard_map/dot_general | solution.py:17
  160.9 0.0 copy-done.7
  160.9 3.4 %fusion.18 = f32[1024,2048]{1,0:T(8,128)S(1)} fusion(bf16[1024,768]{1,0:T(8,128)(2,1)S(1)} %get-tuple-element.26, bf16[768,2048]{1,0:T(8,128)(2,1)S(1)} %copy-done.7), kind=kOutput, calls=%fused_computation.25 | convolution fusion | flops 3221225472 | bytes 13107200 | tf_op jit(solution)/shard_map/dot_general | solution.py:382
  164.3 4.0 %fusion.4 = (f32[1024]{0:T(1024)S(1)}, f32[1024,2048]{1,0:T(8,128)S(1)}) fusion(bf16[1024,2048]{1,0:T(8,128)(2,1)S(1)} %copy-done, f32[1024]{0:T(1024)S(1)} %add_rsqrt_fusion, f32[1024,2048]{1,0:T(8,128)S(1)} %fusion.18, bf16[1024,768]{1,0:T(8,128)(2,1)S(1)} %get-tuple-element.25, bf16[768,2048]{1,0:T(8,128)(2,1)S(1)} %copy-done.1, f32[2048]{0:T(1024)S(1)} %copy-done.4), kind=kOutput, calls=%fused_computation.6 | convolution fusion | flops 3233807360 | bytes 25706496 | tf_op jit(solution)/shard_map/dot_general | solution.py:383
  168.4 3.2 %fusion.7.refs_3_ = bf16[1024,2048]{1,0:T(8,128)(2,1)} fusion(f32[1024,2048]{1,0:T(8,128)S(1)} %get-tuple-element.28, bf16[1024,2048]{1,0:T(8,128)(2,1)S(1)} %copy-done, f32[1024]{0:T(1024)S(1)} %broadcast_multiply_fusion, f32[1024]{0:T(1024)S(1)} %add_rsqrt_fusion), kind=kLoop, calls=%fused_computation.9 | loop fusion | flops 12582912 | bytes 16785408 | tf_op jit(solution)/shard_map/convert_element_type | solution.py:384
  171.6 129.5 %reduce.1 = (f32[768,256]{1,0:T(8,128)}, f32[768,256]{1,0:T(8,128)}, f32[768,256]{1,0:T(8,128)}, bf16[1024,512]{1,0:T(8,128)(2,1)}, f32[3,768]{1,0:T(4,128)}) custom-call(bf16[768,2048]{1,0:T(8,128)(2,1)} %multiply_convert_fusion.2.refs_0_, bf16[768,2048]{1,0:T(8,128)(2,1)} %multiply_convert_fusion.1.refs_1_, ...), custom_call_target="tpu_custom_call" | custom-call | tf_op jit(solution)/shard_map/reduce/pallas_call | solution.py:330
  301.1 0.0 copy-start.3
  301.1 0.0 copy-start.2
  301.1 0.0 copy-start.5
  301.1 2.4 copy.16
  303.5 2.1 copy.17
  305.6 0.0 copy-done.3
  305.6 0.9 copy.18
  306.5 0.0 copy-done.2
  306.5 0.9 copy.19
  307.3 0.0 copy-done.5
  307.3 0.6 copy.20
  (2 shorter events, 0.0 us)
Async XLA Ops:
  0.6 130.4 %copy-start.4 = (f32[2048]{0:T(1024)S(1)}, f32[2048]{0:T(1024)}, u32[]{:S(2)}) copy-start(f32[2048]{0:T(1024)} %param.8) | copy-start | bytes 24580
  127.8 3.5 %copy-start = (bf16[1024,2048]{1,0:T(8,128)(2,1)S(1)}, bf16[1024,2048]{1,0:T(8,128)(2,1)}, u32[]{:S(2)}) copy-start(bf16[1024,2048]{1,0:T(8,128)(2,1)} %get-tuple-element.17) | copy-start | bytes 12582916
  131.3 5.6 %copy-start.1 = (bf16[768,2048]{1,0:T(8,128)(2,1)S(1)}, bf16[768,2048]{1,0:T(8,128)(2,1)}, u32[]{:S(2)}) copy-start(bf16[768,2048]{1,0:T(8,128)(2,1)} %get-tuple-element.18) | copy-start | bytes 9437188
  136.9 3.5 %copy-start.6 = (bf16[1024,2048]{1,0:T(8,128)(2,1)S(1)}, bf16[1024,2048]{1,0:T(8,128)(2,1)}, u32[]{:S(2)}) copy-start(bf16[1024,2048]{1,0:T(8,128)(2,1)} %get-tuple-element.15) | copy-start | bytes 12582916
  136.9 3.5 %copy-start.8 = (bf16[768,2048]{1,0:T(8,128)(2,1)S(1)}, bf16[768,2048]{1,0:T(8,128)(2,1)}, u32[]{:S(2)}) copy-start(bf16[768,2048]{1,0:T(8,128)(2,1)} %get-tuple-element.16) | copy-start | bytes 9437188
  155.6 5.3 %copy-start.7 = (bf16[768,2048]{1,0:T(8,128)(2,1)S(1)}, bf16[768,2048]{1,0:T(8,128)(2,1)}, u32[]{:S(2)}) copy-start(bf16[768,2048]{1,0:T(8,128)(2,1)} %get-tuple-element.19) | copy-start | bytes 9437188
  301.1 4.5 %copy-start.3 = (f32[768,256]{1,0:T(8,128)S(1)}, f32[768,256]{1,0:T(8,128)}, u32[]{:S(2)}) copy-start(f32[768,256]{1,0:T(8,128)} %get-tuple-element.36) | copy-start | bytes 2359300
  301.1 5.3 %copy-start.2 = (f32[768,256]{1,0:T(8,128)S(1)}, f32[768,256]{1,0:T(8,128)}, u32[]{:S(2)}) copy-start(f32[768,256]{1,0:T(8,128)} %get-tuple-element.37) | copy-start | bytes 2359300
  301.1 6.2 %copy-start.5 = (f32[3,768]{1,0:T(4,128)S(1)}, f32[3,768]{1,0:T(4,128)}, u32[]{:S(2)}) copy-start(f32[3,768]{1,0:T(4,128)} %get-tuple-element.38) | copy-start | bytes 27652

commit v2 on v1

--- a/solution.py
+++ b/solution.py
@@ -87,10 +87,25 @@
     for a in acts:
         for r in range(1, ny):
             go(remote(small[a], block_of(full[a], tp, width[a]), ys.at[a, r], yr.at[a, r], y_dev(r)))
-    z_order = [r for r in range(2, nz)] + [1] if nz > 1 else []
+    def along(way, m, d):
+        origin = lax.rem(z + nz - way * (d - 1), nz) * nx + x
+        block = block_of(full[m], origin, width[m])
+        lane = (1 - way) // 2
+        return remote(
+            small[m] if d == 1 else block, block, zs.at[lane, m - 2, d], zr.at[lane, m - 2, d],
+            {"fs": lax.rem(z + nz + way, nz) * nx + x},
+        )
+
+    def has_next(way):
+        return z + 1 < nz if way == 1 else z >= 1
+
+    def has_back(way, d):
+        return z >= d if way == 1 else z + d < nz
+
     for m in mats:
-        for r in z_order:
-            go(remote(small[m], block_of(full[m], fs, width[m]), zs.at[m - 2, r], zr.at[m - 2, r], z_dev(r)))
+        for way in (1, -1):
+            if nz > 1:
+                pl.when(has_next(way))(along(way, m, 1).start)
         for q in range(1, nx):
             go(remote(small[m], block_of(full[m], fs, width[m]), xs.at[m - 2, 0, q], xr.at[m - 2, 0, q], x_dev(q)))
     for a in acts:
@@ -113,19 +128,25 @@
         for q in range(1, nc):
             go(remote(block, block, cs.at[a, r, q], cr.at[a, r, q], c_dev(q)))
 
-    def from_z(m, r):
-        origin = lax.rem(z + nz - r, nz) * nx + x
+    def from_z(way, m, d):
+        origin = lax.rem(z + nz - way * d, nz) * nx + x
         block = block_of(full[m], origin, width[m])
-        remote(block, block, zs.at[m - 2, r], zr.at[m - 2, r], z_dev(r)).wait_recv()
+        lane = (1 - way) // 2
+        r = d if way == 1 else nz - d
+        target = {"fs": lax.rem(z + nz + way, nz) * nx + x}
+        remote(block, block, zs.at[lane, m - 2, d], zr.at[lane, m - 2, d], target).wait_recv()
+        if d + 1 < nz:
+            pl.when(has_next(way))(along(way, m, d + 1).start)
         for q in range(1, nx):
-            go(remote(block, block, xs.at[m - 2, r, q], xr.at[m - 2, r, q], x_dev(q)))
+            remote(block, block, xs.at[m - 2, r, q], xr.at[m - 2, r, q], x_dev(q)).start()
 
     late = [(a, r) for a in acts for r in range(1, ny)]
-    for m in mats:
-        for r in z_order:
-            from_z(m, r)
-        if late:
-            from_y(*late.pop(0))
+    for d in range(1, nz):
+        for m in mats:
+            for way in (1, -1):
+                pl.when(has_back(way, d))(functools.partial(from_z, way, m, d))
+            if late:
+                from_y(*late.pop(0))
     for a, r in late:
         from_y(a, r)
     for m in mats:
@@ -142,6 +163,15 @@
                 remote(block, block, cs.at[a, r, q], cr.at[a, r, q], c_dev(q)).wait_recv()
     for store in stores:
         store.wait()
+    for m in mats:
+        for d in range(1, nz):
+            for way in (1, -1):
+                sent = has_next(way) if d == 1 else has_next(way) & has_back(way, d - 1)
+                pl.when(sent)(along(way, m, d).wait_send)
+            origin = lax.rem(z + nz - d, nz) * nx + x
+            block = block_of(full[m], origin, width[m])
+            for q in range(1, nx):
+                remote(block, block, xs.at[m - 2, d, q], xr.at[m - 2, d, q], x_dev(q)).wait_send()
     for copy in sends:
         copy.wait_send()
 
@@ -162,7 +192,7 @@
         out_specs=[ANY] * 5,
         scratch_shapes=[pltpu.VMEM(a.shape, a.dtype) for a in arrays]
         + [
-            dma((5,)), dma((5,)), dma((3, nz)), dma((3, nz)), dma((3, nz, nx)), dma((3, nz, nx)),
+            dma((5,)), dma((5,)), dma((2, 3, nz)), dma((2, 3, nz)), dma((3, nz, nx)), dma((3, nz, nx)),
             dma((2, ny)), dma((2, ny)), dma((2, ny, nc)), dma((2, ny, nc)),
         ],
         compiler_params=pltpu.CompilerParams(collective_id=0, has_side_effects=True),
@@ -177,7 +207,7 @@
     nz, nx, ny, nc = dims
     terms, part, grad = refs[:3], refs[3], refs[4]
     outs, out_x, out_sq = refs[5:8], refs[8], refs[9]
-    (own, x_in, z_out, z_in, p_own, c_in, y_out, y_in, sq_out, sq_in,
+    (own, x_in, z_out, up_in, down_in, p_own, c_in, y_out, y_in, sq_out, sq_in,
      own_sem, p_sem, xs, xr, zs, zr, cs, cr, ys, yr, qs, qr) = refs[10:]
     n_fs = nz * nx
     fs, tp = lax.axis_index("fs"), lax.axis_index("tp")
@@ -210,24 +240,39 @@
         copy.start()
         sends.append(copy)
 
-    z_order = ([r for r in range(2, nz)] + [1] if nz > 1 else []) + [0]
+    z_in = {1: up_in, -1: down_in}
+
+    def has_next(way, d=1):
+        return z + d < nz if way == 1 else z >= d
+
+    def slot(way, d):
+        return d if way == 1 else nz - d
+
     y_order = [r for r in range(1, ny)] + [0]
     for r in y_order:
         for q in range(1, nc):
             index = lax.rem(y + r, ny) * nc + lax.rem(c + q, nc)
             go(remote(block_of(part, index, cols), c_in.at[r, q - 1], cs.at[r, q], cr.at[r, q], c_dev(q)))
-    for r in z_order:
+    def widely(w, r, q):
+        index = lax.rem(z + r, nz) * nx + lax.rem(x + q, nx)
+        return remote(block_of(terms[w], index, width), x_in.at[w, r, q - 1], xs.at[w, r, q], xr.at[w, r, q], x_dev(q))
+
+    def widely_all(r):
         for w in range(3):
             for q in range(1, nx):
-                index = lax.rem(z + r, nz) * nx + lax.rem(x + q, nx)
-                go(remote(block_of(terms[w], index, width), x_in.at[w, r, q - 1], xs.at[w, r, q], xr.at[w, r, q], x_dev(q)))
+                widely(w, r, q).start()
+
+    for d in range(nz - 1, 0, -1):
+        for way in (1, -1):
+            pl.when(has_next(way, d))(functools.partial(widely_all, slot(way, d)))
+    widely_all(0)
     p_loads = {}
     for r in y_order:
         index = lax.rem(y + r, ny) * nc + c
         p_loads[r] = pltpu.make_async_copy(block_of(part, index, cols), p_own.at[r], p_sem.at[r])
         p_loads[r].start()
     loads = {}
-    for r in z_order:
+    for r in range(nz):
         for w in range(3):
             loads[w, r] = pltpu.make_async_copy(block_of(terms[w], z_index(r), width), own.at[w, r], own_sem.at[w, r])
             loads[w, r].start()
@@ -263,18 +308,53 @@
 
         tiles(n_rows, add_pair)
         go(remote(y_out.at[r], y_in.at[r], ys.at[r], yr.at[r], y_dev(r)))
-    for r in z_order[:-1]:
-        for w in range(3):
-            wide_wait(w, r)
-
-            def add_wide(rows):
-                acc = own[w, r, rows, :].astype(f32)
-                for q in range(1, nx):
-                    acc = acc + x_in[w, r, q - 1, rows, :].astype(f32)
-                z_out[w, r, rows, :] = acc.astype(bf16)
-
-            tiles(n_hid, add_wide)
-            go(remote(z_out.at[w, r], z_in.at[w, r], zs.at[w, r], zr.at[w, r], {"fs": z_index(r)}))
+    def along(way, w, d):
+        r = slot(way, d)
+        lane = (1 - way) // 2
+        return remote(
+            z_out.at[w, r], z_in[way].at[w, d - 1], zs.at[w, r], zr.at[lane, w, d - 1],
+            {"fs": lax.rem(z + nz + way, nz) * nx + x},
+        )
+
+    def arrive(way, w, d):
+        lane = (1 - way) // 2
+        remote(
+            z_out.at[w, 0], z_in[way].at[w, d], zs.at[w, 0], zr.at[lane, w, d],
+            {"fs": lax.rem(z + nz + way, nz) * nx + x},
+        ).wait_recv()
+
+    def clear(way):
+        def rows_clear(rows):
+            for w in range(3):
+                for d in range(nz):
+                    z_in[way][w, d, rows, :] = jnp.zeros((rows.size, width), bf16)
+
+        tiles(n_hid, rows_clear)
+
+    pl.when(z == 0)(functools.partial(clear, 1))
+    pl.when(z == nz - 1)(functools.partial(clear, -1))
+
+    def pass_on(way, w, d):
+        r = slot(way, d)
+        wide_wait(w, r)
+        if d < nz - 1:
+            pl.when(has_next(-way))(functools.partial(arrive, way, w, d))
+
+        def add_wide(rows):
+            acc = own[w, r, rows, :].astype(f32)
+            for q in range(1, nx):
+                acc = acc + x_in[w, r, q - 1, rows, :].astype(f32)
+            if d < nz - 1:
+                acc = acc + z_in[way][w, d, rows, :].astype(f32)
+            z_out[w, r, rows, :] = acc.astype(bf16)
+
+        tiles(n_hid, add_wide)
+        along(way, w, d).start()
+
+    for d in range(nz - 1, 0, -1):
+        for way in (1, -1):
+            for w in range(3):
+                pl.when(has_next(way, d))(functools.partial(pass_on, way, w, d))
     pair_wait(0)
     for r in range(1, ny):
         remote(y_out.at[r], y_in.at[r], ys.at[r], yr.at[r], y_dev(r)).wait_recv()
@@ -291,15 +371,16 @@
     ones = jnp.ones((8, width), f32)
     for w in range(3):
         wide_wait(w, 0)
-        for r in z_order[:-1]:
-            remote(z_out.at[w, r], z_in.at[w, r], zs.at[w, r], zr.at[w, r], {"fs": z_index(r)}).wait_recv()
+        for way in (1, -1):
+            if nz > 1:
+                pl.when(has_next(-way))(functools.partial(arrive, way, w, 0))
 
         def finish_term(rows):
             acc = own[w, 0, rows, :].astype(f32)
             for q in range(1, nx):
                 acc = acc + x_in[w, 0, q - 1, rows, :].astype(f32)
-            for r in z_order[:-1]:
-                acc = acc + z_in[w, r, rows, :].astype(f32)
+            for way in (1, -1):
+                acc = acc + z_in[way][w, 0, rows, :].astype(f32)
             outs[w][rows, :] = acc
             squares = lax.dot_general(
                 ones, acc * acc, (((1,), (1,)), ((), ())),
@@ -315,6 +396,13 @@
         remote(sq_out, sq_in.at[k], qs.at[k], qr.at[k], fs_dev(k)).wait_recv()
         total = total + sq_in[k]
     out_sq[...] = total / width_total
+    for w in range(3):
+        for r in range(nz):
+            for q in range(1, nx):
+                widely(w, r, q).wait_send()
+        for d in range(1, nz):
+            for way in (1, -1):
+                pl.when(has_next(way, d))(along(way, w, d).wait_send)
     for copy in sends:
         copy.wait_send()
 
@@ -338,6 +426,7 @@
             pltpu.VMEM((3, nz, max(1, nx - 1), hid, width), bf16),
             pltpu.VMEM((3, nz, hid, width), bf16),
             pltpu.VMEM((3, nz, hid, width), bf16),
+            pltpu.VMEM((3, nz, hid, width), bf16),
             pltpu.VMEM((ny, rows, cols), bf16),
             pltpu.VMEM((ny, max(1, nc - 1), rows, cols), bf16),
             pltpu.VMEM((ny, rows, cols), bf16),
@@ -345,7 +434,7 @@
             pltpu.VMEM((3, hid), f32),
             pltpu.VMEM((n_fs, 3, hid), f32),
             dma((3, nz)), dma((ny,)),
-            dma((3, nz, nx)), dma((3, nz, nx)), dma((3, nz)), dma((3, nz)),
+            dma((3, nz, nx)), dma((3, nz, nx)), dma((3, nz)), dma((2, 3, nz)),
             dma((ny, nc)), dma((ny, nc)), dma((ny,)), dma((ny,)),
             dma((n_fs,)), dma((n_fs,)),
         ],

time: 308 us -> 278 us (0.903)
  Pallas kernels: 257 us -> 227 us
    pallas_call x1, Pallas kernels: 130 us -> 113 us  [reduce_all(): pl.pallas_call(functools.partial(reduce_kernel, dims, n_fs * width), out_...]
    pallas_call x1, Pallas kernels: 127 us -> 114 us  [gather_all(): pl.pallas_call(functools.partial(gather_kernel, dims), out_shape=shapes,...]
where the time goes in v2:
time: 278 us
  Pallas kernels  227 us (82%)
  matrix products  37 us (13%)
  local copies, waits for them, and re-layouts  7.03 us (3%)
  other arithmetic  6.44 us (2%)
    pallas_call x1, Pallas kernels, gather_all(): pl.pallas_call(functools.partial(gather_kernel, dims), out_shape=shapes,...  114 us
    pallas_call x1, Pallas kernels, reduce_all(): pl.pallas_call(functools.partial(reduce_kernel, dims, n_fs * width), out_...  113 us
    dot_general x6, matrix products, contract(): lax.dot_general(left, right, (((left_dim,), (right_dim,)), ((), ())), pre...  29.6 us
    unnamed x23, local copies, waits for them, and re-layouts  7.03 us

profile of v2, /device:TPU:0, one launch (start us, length us, event | category | flops | bytes accessed | tf_op | source)
XLA Modules:
  0.0 278.2 jit_solution(4449922068062921031)
XLA Ops:
  0.6 0.0 copy-start.4
  0.6 114.2 %gather.1 = (bf16[1024,2048]{1,0:T(8,128)(2,1)}, bf16[1024,2048]{1,0:T(8,128)(2,1)}, bf16[768,2048]{1,0:T(8,128)(2,1)}, bf16[768,2048]{1,0:T(8,128)(2,1)}, bf16[768,2048]{1,0:T(8,128)(2,1)}) custom-call(bf16[1024,512]{1,0:T(8,128)(2,1)} %refs_0_.1, bf16[1024,512]{1,0:T(8,128)(2,1)} %refs_4_.3, bf16[768,256]{1,0:T(8,128)(2,1)} %refs_2_.1, ...), custom_call_target="tpu_custom_call" | custom-call | tf_op jit(solution)/shard_map/gather/pallas_call | solution.py:188
  114.8 0.0 copy-start
  114.8 3.2 %fusion.8 = f32[1024]{0:T(1024)S(1)} fusion(bf16[1024,2048]{1,0:T(8,128)(2,1)} %get-tuple-element.17), kind=kLoop, calls=%fused_computation.10 | loop fusion | flops 6290432 | bytes 4198400 | tf_op jit(solution)/shard_map/reduce_sum | solution.py:453
  118.1 0.0 copy-done.4
  118.1 0.2 copy-done
  118.3 0.0 copy-start.1
  118.3 5.6 %fusion.14 = f32[1024,768]{1,0:T(8,128)S(1)} fusion(bf16[768,2048]{1,0:T(8,128)(2,1)} %get-tuple-element.19, bf16[1024,2048]{1,0:T(8,128)(2,1)S(1)} %copy-done, f32[2048]{0:T(1024)S(1)} %copy-done.4, f32[1024]{0:T(1024)S(1)} %add_rsqrt_fusion), kind=kOutput, calls=%fused_computation.23 | convolution fusion | flops 3229614080 | bytes 10498048 | tf_op jit(solution)/shard_map/dot_general | solution.py:17
  123.9 0.0 copy-done.1
  123.9 0.0 copy-start.6
  123.9 0.0 copy-start.8
  123.9 3.5 %fusion.16 = f32[1024,768]{1,0:T(8,128)S(1)} fusion(bf16[768,2048]{1,0:T(8,128)(2,1)S(1)} %copy-done.1, bf16[1024,2048]{1,0:T(8,128)(2,1)S(1)} %copy-done, f32[2048]{0:T(1024)S(1)} %copy-done.4, f32[1024]{0:T(1024)S(1)} %add_rsqrt_fusion), kind=kOutput, calls=%fused_computation.24 | convolution fusion | flops 3229614080 | bytes 10498048 | tf_op jit(solution)/shard_map/dot_general | solution.py:17
  127.4 0.0 copy-done.6
  127.4 0.0 copy-done.8
  127.5 4.4 %multiply_convert_fusion.4 = (bf16[1024,768]{1,0:T(8,128)(2,1)S(1)}, bf16[1024,768]{1,0:T(8,128)(2,1)S(1)}) fusion(f32[1024,768]{1,0:T(8,128)S(1)} %fusion.14, f32[1024,768]{1,0:T(8,128)S(1)} %fusion.16, bf16[1024,2048]{1,0:T(8,128)(2,1)S(1)} %copy-done.6, bf16[768,2048]{1,0:T(8,128)(2,1)S(1)} %copy-done.8), kind=kOutput, calls=%fused_computation.16 | convolution fusion | flops 3232235520 | bytes 16777216 | tf_op jit(solution)/shard_map/dot_general | solution.py:17
  131.9 5.4 %multiply_convert_fusion.refs_2_ = bf16[768,2048]{1,0:T(8,128)(2,1)} fusion(bf16[1024,2048]{1,0:T(8,128)(2,1)S(1)} %copy-done.6, f32[1024,768]{1,0:T(8,128)S(1)} %fusion.16, f32[1024,768]{1,0:T(8,128)S(1)} %fusion.14), kind=kOutput, calls=%fused_computation.12 | convolution fusion | flops 3229089792 | bytes 13631488 | tf_op jit(solution)/shard_map/dot_general | solution.py:17
  137.3 5.3 %multiply_convert_fusion.1.refs_1_ = bf16[768,2048]{1,0:T(8,128)(2,1)} fusion(bf16[1024,768]{1,0:T(8,128)(2,1)S(1)} %get-tuple-element.25, bf16[1024,2048]{1,0:T(8,128)(2,1)S(1)} %copy-done, f32[2048]{0:T(1024)S(1)} %copy-done.4, f32[1024]{0:T(1024)S(1)} %add_rsqrt_fusion), kind=kOutput, calls=%fused_computation.13 | convolution fusion | flops 3232759808 | bytes 8925184 | tf_op jit(solution)/shard_map/dot_general | solution.py:17
  142.6 0.0 copy-start.7
  142.6 5.3 %multiply_convert_fusion.2.refs_0_ = bf16[768,2048]{1,0:T(8,128)(2,1)} fusion(bf16[1024,768]{1,0:T(8,128)(2,1)S(1)} %get-tuple-element.26, bf16[1024,2048]{1,0:T(8,128)(2,1)S(1)} %copy-done, f32[2048]{0:T(1024)S(1)} %copy-done.4, f32[1024]{0:T(1024)S(1)} %add_rsqrt_fusion), kind=kOutput, calls=%fused_computation.14 | convolution fusion | flops 3232759808 | bytes 8925184 | tf_op jit(solution)/shard_map/dot_general | solution.py:17
  147.9 0.0 copy-done.7
  147.9 3.4 %fusion.18 = f32[1024,2048]{1,0:T(8,128)S(1)} fusion(bf16[1024,768]{1,0:T(8,128)(2,1)S(1)} %get-tuple-element.26, bf16[768,2048]{1,0:T(8,128)(2,1)S(1)} %copy-done.7), kind=kOutput, calls=%fused_computation.25 | convolution fusion | flops 3221225472 | bytes 13107200 | tf_op jit(solution)/shard_map/dot_general | solution.py:471
  151.4 4.0 %fusion.4 = (f32[1024]{0:T(1024)S(1)}, f32[1024,2048]{1,0:T(8,128)S(1)}) fusion(bf16[1024,2048]{1,0:T(8,128)(2,1)S(1)} %copy-done, f32[1024]{0:T(1024)S(1)} %add_rsqrt_fusion, f32[1024,2048]{1,0:T(8,128)S(1)} %fusion.18, bf16[1024,768]{1,0:T(8,128)(2,1)S(1)} %get-tuple-element.25, bf16[768,2048]{1,0:T(8,128)(2,1)S(1)} %copy-done.1, f32[2048]{0:T(1024)S(1)} %copy-done.4), kind=kOutput, calls=%fused_computation.6 | convolution fusion | flops 3233807360 | bytes 25706496 | tf_op jit(solution)/shard_map/dot_general | solution.py:472
  155.4 3.2 %fusion.7.refs_3_ = bf16[1024,2048]{1,0:T(8,128)(2,1)} fusion(f32[1024,2048]{1,0:T(8,128)S(1)} %get-tuple-element.28, bf16[1024,2048]{1,0:T(8,128)(2,1)S(1)} %copy-done, f32[1024]{0:T(1024)S(1)} %broadcast_multiply_fusion, f32[1024]{0:T(1024)S(1)} %add_rsqrt_fusion), kind=kLoop, calls=%fused_computation.9 | loop fusion | flops 12582912 | bytes 16785408 | tf_op jit(solution)/shard_map/convert_element_type | solution.py:473
  158.6 112.8 %reduce.1 = (f32[768,256]{1,0:T(8,128)}, f32[768,256]{1,0:T(8,128)}, f32[768,256]{1,0:T(8,128)}, bf16[1024,512]{1,0:T(8,128)(2,1)}, f32[3,768]{1,0:T(4,128)}) custom-call(bf16[768,2048]{1,0:T(8,128)(2,1)} %multiply_convert_fusion.2.refs_0_, bf16[768,2048]{1,0:T(8,128)(2,1)} %multiply_convert_fusion.1.refs_1_, ...), custom_call_target="tpu_custom_call" | custom-call | tf_op jit(solution)/shard_map/reduce/pallas_call | solution.py:418
  271.4 0.0 copy-start.3
  271.4 0.0 copy-start.2
  271.4 0.0 copy-start.5
  271.4 2.4 copy.16
  273.8 2.1 copy.17
  275.9 0.0 copy-done.3
  275.9 0.9 copy.18
  276.7 0.0 copy-done.2
  276.8 0.9 copy.19
  277.6 0.0 copy-done.5
  277.6 0.6 copy.20
  (2 shorter events, 0.0 us)
Async XLA Ops:
  0.6 117.4 %copy-start.4 = (f32[2048]{0:T(1024)S(1)}, f32[2048]{0:T(1024)}, u32[]{:S(2)}) copy-start(f32[2048]{0:T(1024)} %param.8) | copy-start | bytes 24580
  114.8 3.5 %copy-start = (bf16[1024,2048]{1,0:T(8,128)(2,1)S(1)}, bf16[1024,2048]{1,0:T(8,128)(2,1)}, u32[]{:S(2)}) copy-start(bf16[1024,2048]{1,0:T(8,128)(2,1)} %get-tuple-element.17) | copy-start | bytes 12582916
  118.3 5.6 %copy-start.1 = (bf16[768,2048]{1,0:T(8,128)(2,1)S(1)}, bf16[768,2048]{1,0:T(8,128)(2,1)}, u32[]{:S(2)}) copy-start(bf16[768,2048]{1,0:T(8,128)(2,1)} %get-tuple-element.18) | copy-start | bytes 9437188
  123.9 3.5 %copy-start.6 = (bf16[1024,2048]{1,0:T(8,128)(2,1)S(1)}, bf16[1024,2048]{1,0:T(8,128)(2,1)}, u32[]{:S(2)}) copy-start(bf16[1024,2048]{1,0:T(8,128)(2,1)} %get-tuple-element.15) | copy-start | bytes 12582916
  123.9 3.5 %copy-start.8 = (bf16[768,2048]{1,0:T(8,128)(2,1)S(1)}, bf16[768,2048]{1,0:T(8,128)(2,1)}, u32[]{:S(2)}) copy-start(bf16[768,2048]{1,0:T(8,128)(2,1)} %get-tuple-element.16) | copy-start | bytes 9437188
  142.6 5.3 %copy-start.7 = (bf16[768,2048]{1,0:T(8,128)(2,1)S(1)}, bf16[768,2048]{1,0:T(8,128)(2,1)}, u32[]{:S(2)}) copy-start(bf16[768,2048]{1,0:T(8,128)(2,1)} %get-tuple-element.19) | copy-start | bytes 9437188
  271.4 4.5 %copy-start.3 = (f32[768,256]{1,0:T(8,128)S(1)}, f32[768,256]{1,0:T(8,128)}, u32[]{:S(2)}) copy-start(f32[768,256]{1,0:T(8,128)} %get-tuple-element.36) | copy-start | bytes 2359300
  271.4 5.3 %copy-start.2 = (f32[768,256]{1,0:T(8,128)S(1)}, f32[768,256]{1,0:T(8,128)}, u32[]{:S(2)}) copy-start(f32[768,256]{1,0:T(8,128)} %get-tuple-element.37) | copy-start | bytes 2359300
  271.4 6.2 %copy-start.5 = (f32[3,768]{1,0:T(4,128)S(1)}, f32[3,768]{1,0:T(4,128)}, u32[]{:S(2)}) copy-start(f32[3,768]{1,0:T(4,128)} %get-tuple-element.38) | copy-start | bytes 27652
